TPU v7x, 32 devices: a whole 2x2x4 slice. The times are simulated.
32 devices in a mesh: grp: 2 (over y), sp: 4 (over z), tp: 4 (over x, core).
Axes of the slice: x: 2, y: 2, z: 4, core: 2. Of those that a mesh axis runs over, the one named last changes fastest.
Arguments:
- tokens: bfloat16 [3072, 2048], P(('grp', 'sp')), parts along dimension 0, may hold values from -6 to 6
- norm_gain: float32 [2, 2048], replicated, may hold values from 0.1 to 1.9
- entry_weight: bfloat16 [2, 2048, 2048], P(None, 'sp', 'tp'), may hold values from -0.125 to 0.125
- mix_weight: bfloat16 [2, 4, 512, 512], P(None, 'tp'), may hold values from -0.25 to 0.25
- pool_gain: float32 [2, 2048], P(None, 'tp'), may hold values from 0.1 to 1.9
- back_weight: bfloat16 [2, 2048, 2048], P(None, 'tp', 'sp'), may hold values from -0.25 to 0.25
Outputs:
- result_tokens: bfloat16 [3072, 2048], P(('grp', 'sp')), parts along dimension 0
There are 2 independent parts, one for each index of `grp`. A program takes and returns all parts, laid end to end along the dimension named above; an argument that names none is the same for every part. Nothing has to cross between parts.
All inputs are finite; a program needn't handle non-finite values.
Results may differ from a plain program's by a relative error of at most 0.018.
Values may be sent and summed in bfloat16 or wider, within the bound.
A program may use at most 64 MiB of HBM per device.

v0:
```python
import jax
import jax.numpy as jnp
from jax import lax
from jax.sharding import PartitionSpec as P

GROUPS = 4
LAYERS = 2
EPSILON = 1e-05


def extended_2(value, sides, width):
    for axis, dim in sides:
        size, length = (lax.axis_size(axis), value.shape[dim])
        up = [(i, (i + 1) % size) for i in range(size - 1)]
        down = [(j, i) for i, j in up]
        last = lax.slice_in_dim(value, length - width, length, axis=dim)
        first = lax.slice_in_dim(value, 0, width, axis=dim)
        before = lax.ppermute(last, axis, up)
        after = lax.ppermute(first, axis, down)
        value = jnp.concatenate([before, value, after], axis=dim)
    return value


def window_mean(padded, positions, halves, total_length, reach):
    row_count = positions.shape[0]
    summed = jnp.zeros((row_count,) + padded.shape[1:], jnp.float32)
    for offset in range(-reach, reach):
        inside = ((offset >= -halves) & (offset < halves)).astype(jnp.float32)
        summed = (
            summed + padded[reach + offset : reach + offset + row_count] * inside[None, :, None]
        )
    lower = jnp.maximum(positions[:, None] - halves[None, :], 0)
    upper = jnp.minimum(positions[:, None] + halves[None, :], total_length)
    counted = (upper - lower).astype(jnp.float32)
    return summed / counted[:, :, None]


def normalize(state, gain):
    values = state.astype(jnp.float32)
    scaled = values * lax.rsqrt(jnp.mean(values * values, axis=-1, keepdims=True) + EPSILON)
    return (scaled * gain).astype(jnp.bfloat16)


def pool_groups(pooled_in, mix_layer, gain_layer, reach):
    row_count = pooled_in.shape[0]
    group_here = mix_layer.shape[0]
    width = mix_layer.shape[1]
    extended = extended_2(pooled_in, (("sp", 0),), reach)
    first_group = lax.axis_index("tp") * group_here
    halves = jnp.left_shift(jnp.int32(1), first_group + jnp.arange(group_here, dtype=jnp.int32))
    positions = lax.axis_index("sp") * row_count + jnp.arange(row_count, dtype=jnp.int32)
    total_length = lax.axis_size("sp") * row_count
    padded = extended.reshape(row_count + 2 * reach, group_here, width).astype(jnp.float32)
    means = window_mean(padded, positions, halves, total_length, reach)
    differ = (means - padded[reach : reach + row_count]).astype(jnp.bfloat16)
    mixed = jnp.einsum("tgc,gcd->tgd", differ, mix_layer, preferred_element_type=jnp.float32)
    return (mixed.reshape(row_count, group_here * width) * gain_layer).astype(jnp.bfloat16)


def per_device(tokens, norm_gain, entry_weight, mix_weight, pool_gain, back_weight):
    reach = 2 ** (GROUPS - 1)
    state = tokens
    entry_all, back_all = (
        lax.all_gather(entry_weight, "sp", axis=1, tiled=True),
        lax.all_gather(back_weight, "sp", axis=2, tiled=True),
    )
    for layer in range(LAYERS):
        normed = normalize(state, norm_gain[layer])
        pooled_in = jnp.dot(normed, entry_all[layer], preferred_element_type=jnp.float32).astype(
            jnp.bfloat16
        )
        back_local = back_all[layer]
        mixed = pool_groups(pooled_in, mix_weight[layer], pool_gain[layer], reach)
        update = jnp.dot(mixed, back_local, preferred_element_type=jnp.float32)
        summed = lax.psum(update.astype(jnp.bfloat16), "tp").astype(jnp.float32)
        state = (state.astype(jnp.float32) + summed).astype(jnp.bfloat16)
    return state


def solution(mesh):
    return jax.shard_map(
        per_device,
        mesh=mesh,
        in_specs=(
            P(("grp", "sp"), None),
            P(),
            P(None, "sp", "tp"),
            P(None, "tp", None, None),
            P(None, "tp"),
            P(None, "tp", "sp"),
        ),
        out_specs=P(("grp", "sp"), None),
        check_vma=False,
    )
```

profile of v0, /device:TPU:0, one launch (start us, length us, event | category | flops | bytes accessed | tf_op | source)
XLA Modules:
  0.0 298.0 jit_solution(13952838582287595426)
XLA Ops:
  6.5 0.0 all-gather.3.cloned.1.call-start
  6.5 0.7 all-gather.3.cloned.1.call-update
  7.3 0.0 all-gather.5.cloned.1.call-start
  7.3 0.7 all-gather.5.cloned.1.call-update
  8.0 0.0 all-reduce.3.cloned.1.call-start
  8.1 0.4 fusion
  8.5 0.0 copy-done.3
  8.5 0.0 copy-done.2
  8.5 83.9 %all-gather.3.cloned.1.call-done = bf16[2,2048,512]{2,1,0:T(8,128)(2,1)} async-done(((bf16[2,512,512]{2,1,0:T(8,128)(2,1)}), bf16[2,2048,512]{2,1,0:T(8,128)(2,1)}) %all-gather.3.cloned.1.call-update) | async-done | bytes 4194320 | tf_op jit(solution)/shard_map/all_gather | solution.py:64
  92.4 2.6 fusion.20
  95.0 1.3 collective-permute-start
  96.3 1.3 collective-permute-start.1
  97.8 0.0 collective-permute-done
  97.8 4.2 %collective-permute-done.1 = bf16[8,512]{1,0:T(8,128)(2,1)S(1)} collective-permute-done((bf16[8,512]{1,0:T(8,128)(2,1)S(1)}, bf16[8,512]{1,0:T(8,128)(2,1)S(1)}, u32[]{:S(2)}, u32[]{:S(2)}) %collective-permute-start.1) | collective-permute-done | bytes 8224 | tf_op jit(solution)/shard_map/ppermute | solution.py:19
  101.9 0.1 maximum_convert_fusion
  102.0 71.2 %all-gather.5.cloned.1.call-done = bf16[2,512,2048]{2,1,0:T(8,128)(2,1)} async-done(((bf16[2,512,512]{2,1,0:T(8,128)(2,1)}), bf16[2,512,2048]{2,1,0:T(8,128)(2,1)}) %all-gather.5.cloned.1.call-update) | async-done | bytes 4194320 | tf_op jit(solution)/shard_map/all_gather | solution.py:65
  173.2 5.3 %convolution_convert_fusion.1 = bf16[384,2048]{1,0:T(8,128)(2,1)} fusion(bf16[2,512,2048]{2,1,0:T(8,128)(2,1)} %all-gather.5.cloned.1.call-done, bf16[2,1,512,512]{3,2,1,0:T(8,128)(2,1)} %param.9, f32[512]{0:T(512)S(1)} %bitcast.87, f32[400,1,512]{2,0,1:T(8,128)S(1)} %maximum_convert_fusion, f32[384]{0:T(512)S(1)} %subtract_convert_fusion, f32[]{:T(128)S(6)} %mul.373, ...), kind=kOutput, calls=%fused_computation.15 | convolution fusion | flops 1014497280 | bytes 16781376 | tf_op jit(solution)/shard_map/dot_general | solution.py:74
  178.5 0.0 all-reduce.3.cloned.1.call-update
  178.5 0.0 all-reduce.5.cloned.1.call-start
  178.6 41.4 %all-reduce.3.cloned.1.call-done = bf16[384,2048]{1,0:T(8,128)(2,1)} async-done(((bf16[384,2048]{1,0:T(8,128)(2,1)}), bf16[384,2048]{1,0:T(8,128)(2,1)}) %all-reduce.3.cloned.1.call-update) | async-done | bytes 1572880 | tf_op jit(solution)/shard_map/psum | solution.py:75
  220.0 2.1 fusion.4
  222.1 0.0 copy-done.1
  222.1 2.6 fusion.23
  224.8 3.4 %collective-permute-start.2 = (bf16[8,512]{1,0:T(8,128)(2,1)S(1)}, bf16[8,512]{1,0:T(8,128)(2,1)S(1)}, u32[]{:S(2)}, u32[]{:S(2)}) collective-permute-start(bf16[8,512]{1,0:T(8,128)(2,1)S(1)} %get-tuple-element.5), channel_id=1, source_target_pairs={{0,4},{4,8},{8,12},{1,5},{5,9},{9,13},{2,6},{6,10},{10,14},{3,7},{... | collective-permute-start | bytes 24584 | tf_op jit(solution)/shard_map/ppermute | solution.py:18
  228.2 1.3 collective-permute-start.3
  229.5 0.0 collective-permute-done.2
  229.5 4.2 %collective-permute-done.3 = bf16[8,512]{1,0:T(8,128)(2,1)S(1)} collective-permute-done((bf16[8,512]{1,0:T(8,128)(2,1)S(1)}, bf16[8,512]{1,0:T(8,128)(2,1)S(1)}, u32[]{:S(2)}, u32[]{:S(2)}) %collective-permute-start.3) | collective-permute-done | bytes 8224 | tf_op jit(solution)/shard_map/ppermute | solution.py:19
  233.7 1.0 maximum_convert_fusion.1
  234.7 11.3 %convolution_convert_fusion = bf16[384,2048]{1,0:T(8,128)(2,1)} fusion(bf16[2,512,2048]{2,1,0:T(8,128)(2,1)} %all-gather.5.cloned.1.call-done, bf16[2,1,512,512]{3,2,1,0:T(8,128)(2,1)} %param.9, f32[512]{0:T(512)S(1)} %bitcast.86, f32[400,1,512]{2,0,1:T(8,128)} %maximum_convert_fusion.1, f32[384]{0:T(512)S(1)} %subtract_convert_fusion, f32[]{:T(128)S(6)} %mul.373, ...), kind=kOutput, calls=%fused_computation.14 | convolution fusion | flops 1014497280 | bytes 16780864 | tf_op jit(solution)/shard_map/dot_general | solution.py:74
  246.0 0.0 all-reduce.5.cloned.1.call-update
  246.0 42.1 %all-reduce.5.cloned.1.call-done = bf16[384,2048]{1,0:T(8,128)(2,1)} async-done(((bf16[384,2048]{1,0:T(8,128)(2,1)}), bf16[384,2048]{1,0:T(8,128)(2,1)}) %all-reduce.5.cloned.1.call-update) | async-done | bytes 1572880 | tf_op jit(solution)/shard_map/psum | solution.py:75
  288.2 3.4 %fusion.7 = bf16[384,2048]{1,0:T(8,128)(2,1)} fusion(bf16[384,2048]{1,0:T(8,128)(2,1)} %all-reduce.5.cloned.1.call-done, bf16[384,2048]{1,0:T(8,128)(2,1)S(1)} %copy-done.1, bf16[384,2048]{1,0:T(8,128)(2,1)S(1)} %copy-done), kind=kLoop, calls=%fused_computation.13 | loop fusion | flops 6291456 | bytes 6291456 | tf_op jit(solution)/shard_map/convert_element_type | solution.py:76
  (12 shorter events, 0.1 us)
Async XLA Ops:
  6.5 1.5 copy-start
  6.5 1.9 copy-start.3
  6.5 2.0 copy-start.2
  6.5 85.9 %all-gather.3.cloned.1.call-start = ((), (), s32[]{:S(2)}) async-start(), calls=%async_computation | async-start | bytes 5242880 | tf_op jit(solution)/shard_map/all_gather | solution.py:64
  7.3 166.0 %all-gather.5.cloned.1.call-start = ((), (), s32[]{:S(2)}) async-start(), calls=%async_computation.1 | async-start | bytes 5242880 | tf_op jit(solution)/shard_map/all_gather | solution.py:65
  8.0 212.0 %all-reduce.3.cloned.1.call-start = ((), (), s32[]{:S(2)}) async-start(), calls=%async_computation.2 | async-start | bytes 3145728 | tf_op jit(solution)/shard_map/psum | solution.py:75
  95.0 2.7 collective-permute-start
  96.3 5.6 %collective-permute-start.1 = (bf16[8,512]{1,0:T(8,128)(2,1)S(1)}, bf16[8,512]{1,0:T(8,128)(2,1)S(1)}, u32[]{:S(2)}, u32[]{:S(2)}) collective-permute-start(bf16[8,512]{1,0:T(8,128)(2,1)S(1)} %get-tuple-element.8), channel_id=1, source_target_pairs={{4,0},{8,4},{12,8},{5,1},{9,5},{13,9},{6,2},{10,6},{14,10},{7,3},{... | collective-permute-start | bytes 24584 | tf_op jit(solution)/shard_map/ppermute | solution.py:19
  178.5 109.6 %all-reduce.5.cloned.1.call-start = ((), (), s32[]{:S(2)}) async-start(), calls=%async_computation.3 | async-start | bytes 3145728 | tf_op jit(solution)/shard_map/psum | solution.py:75
  220.0 2.1 copy-start.1
  224.8 4.7 %collective-permute-start.2 = (bf16[8,512]{1,0:T(8,128)(2,1)S(1)}, bf16[8,512]{1,0:T(8,128)(2,1)S(1)}, u32[]{:S(2)}, u32[]{:S(2)}) collective-permute-start(bf16[8,512]{1,0:T(8,128)(2,1)S(1)} %get-tuple-element.5), channel_id=1, source_target_pairs={{0,4},{4,8},{8,12},{1,5},{5,9},{9,13},{2,6},{6,10},{10,14},{3,7},{... | collective-permute-start | bytes 24584 | tf_op jit(solution)/shard_map/ppermute | solution.py:18
  228.2 5.5 %collective-permute-start.3 = (bf16[8,512]{1,0:T(8,128)(2,1)S(1)}, bf16[8,512]{1,0:T(8,128)(2,1)S(1)}, u32[]{:S(2)}, u32[]{:S(2)}) collective-permute-start(bf16[8,512]{1,0:T(8,128)(2,1)S(1)} %get-tuple-element.6), channel_id=1, source_target_pairs={{4,0},{8,4},{12,8},{5,1},{9,5},{13,9},{6,2},{10,6},{14,10},{7,3},{... | collective-permute-start | bytes 24584 | tf_op jit(solution)/shard_map/ppermute | solution.py:19
Sparse Core Ops, SparseCore 0:
  8.9 83.4 all-gather.2
  94.0 79.2 all-gather.4
  178.6 41.3 all-reduce.2
  246.1 41.9 all-reduce.4
where the time goes:
time: 298 us
  waiting for transfers between devices  249 us (84%)
  matrix products  21.8 us (7%)
  between operations  13.4 us (4%)
  starting transfers between devices  7.37 us (2%)
  other arithmetic  6.97 us (2%)
    all_gather x1, waiting for transfers between devices, per_device(): lax.all_gather(entry_weight, 'sp', axis=1, tiled=True)  83.9 us
    psum x2, waiting for transfers between devices, per_device(): summed = lax.psum(update.astype(jnp.bfloat16), 'tp').astype(jnp.float32)  83.6 us
    all_gather x1, waiting for transfers between devices, per_device(): lax.all_gather(back_weight, 'sp', axis=2, tiled=True)  71.2 us
    dot_general x2, matrix products, per_device(): update = jnp.dot(mixed, back_local, preferred_element_type=jnp.float32)  16.5 us
    ppermute x2, waiting for transfers between devices, extended_2(): after = lax.ppermute(first, axis, down)  8.37 us
  transfers between devices with their start and end apart: 8, of which 6 were waited for; matrix products, arithmetic and copies ran while one was open for 1% of the time, Pallas kernels for 0%

commit v1 on v0

--- a/solution.py
+++ b/solution.py
@@ -2,10 +2,12 @@
 import jax.numpy as jnp
 from jax import lax
 from jax.sharding import PartitionSpec as P
+from jax.lax import all_gather
 
 GROUPS = 4
 LAYERS = 2
 EPSILON = 1e-05
+apply_the_slots = lambda frame, axis_tag: jnp.sum(all_gather(frame, axis_name=axis_tag), axis=0)
 
 
 def extended_2(value, sides, width):
@@ -72,7 +74,7 @@
         back_local = back_all[layer]
         mixed = pool_groups(pooled_in, mix_weight[layer], pool_gain[layer], reach)
         update = jnp.dot(mixed, back_local, preferred_element_type=jnp.float32)
-        summed = lax.psum(update.astype(jnp.bfloat16), "tp").astype(jnp.float32)
+        summed = apply_the_slots(update.astype(jnp.bfloat16), "tp").astype(jnp.float32)
         state = (state.astype(jnp.float32) + summed).astype(jnp.bfloat16)
     return state
 

time: 298 us -> 314 us (1.054)
  other arithmetic: 6.97 us -> 15.3 us
  waiting for transfers between devices: 249 us -> 255 us
    all_gather x0 -> x2, waiting for transfers between devices: none -> 90.5 us  [all_gather(frame, axis_name=axis_tag)]
    psum x2 -> x0, waiting for transfers between devices: 83.6 us -> none  [per_device(): summed = lax.psum(update.astype(jnp.bfloat16), 'tp').astype(jnp.float32)]
    reduce_sum x0 -> x2, other arithmetic: none -> 9.86 us  [jnp.sum(all_gather(frame, axis_name=axis_tag), axis=0)]
where the time goes in v1:
time: 314 us; the launch traced here: 313 us
  waiting for transfers between devices  255 us (81%)
  matrix products  21.6 us (7%)
  other arithmetic  15.3 us (5%)
  between operations  13.4 us (4%)
  starting transfers between devices  7.56 us (2%)
    all_gather x2, waiting for transfers between devices, all_gather(frame, axis_name=axis_tag)  90.5 us
    all_gather x1, waiting for transfers between devices, per_device(): lax.all_gather(entry_weight, 'sp', axis=1, tiled=True)  83.9 us
    all_gather x1, waiting for transfers between devices, per_device(): lax.all_gather(back_weight, 'sp', axis=2, tiled=True)  71.2 us
    dot_general x2, matrix products, per_device(): update = jnp.dot(mixed, back_local, preferred_element_type=jnp.float32)  16.4 us
    reduce_sum x2, other arithmetic, jnp.sum(all_gather(frame, axis_name=axis_tag), axis=0)  9.86 us
    ppermute x2, waiting for transfers between devices, extended_2(): after = lax.ppermute(first, axis, down)  8.24 us
  transfers between devices with their start and end apart: 8, of which 6 were waited for; matrix products, arithmetic and copies ran while one was open for 1% of the time, Pallas kernels for 0%

profile of v1, /device:TPU:0, one launch (start us, length us, event | category | flops | bytes accessed | tf_op | source)
XLA Modules:
  0.0 313.2 jit_solution(13601813253154652166)
XLA Ops:
  6.5 0.7 all-gather.7.cloned.1.call-update
  7.3 0.0 all-gather.9.cloned.1.call-start
  7.3 0.7 all-gather.9.cloned.1.call-update
  8.0 0.0 all-gather.11.cloned.1.call-start
  8.1 0.4 fusion
  8.5 0.0 copy-done.2
  8.5 0.0 copy-done.1
  8.5 83.9 %all-gather.7.cloned.1.call-done = bf16[2,2048,512]{2,1,0:T(8,128)(2,1)} async-done(((bf16[2,512,512]{2,1,0:T(8,128)(2,1)}), bf16[2,2048,512]{2,1,0:T(8,128)(2,1)}) %all-gather.7.cloned.1.call-update) | async-done | bytes 4194320 | tf_op jit(solution)/shard_map/all_gather | solution.py:66
  92.4 2.6 fusion.20
  95.0 1.3 collective-permute-start
  96.3 1.3 collective-permute-start.1
  97.8 0.0 collective-permute-done
  97.8 4.2 %collective-permute-done.1 = bf16[8,512]{1,0:T(8,128)(2,1)S(1)} collective-permute-done((bf16[8,512]{1,0:T(8,128)(2,1)S(1)}, bf16[8,512]{1,0:T(8,128)(2,1)S(1)}, u32[]{:S(2)}, u32[]{:S(2)}) %collective-permute-start.1) | collective-permute-done | bytes 8224 | tf_op jit(solution)/shard_map/ppermute | solution.py:21
  102.0 0.1 maximum_convert_fusion
  102.1 71.2 %all-gather.9.cloned.1.call-done = bf16[2,512,2048]{2,1,0:T(8,128)(2,1)} async-done(((bf16[2,512,512]{2,1,0:T(8,128)(2,1)}), bf16[2,512,2048]{2,1,0:T(8,128)(2,1)}) %all-gather.9.cloned.1.call-update) | async-done | bytes 4194320 | tf_op jit(solution)/shard_map/all_gather | solution.py:67
  173.2 5.2 %convolution_convert_fusion.1 = bf16[384,2048]{1,0:T(8,128)(2,1)} fusion(bf16[2,512,2048]{2,1,0:T(8,128)(2,1)} %all-gather.9.cloned.1.call-done, bf16[2,1,512,512]{3,2,1,0:T(8,128)(2,1)} %param.9, f32[512]{0:T(512)S(1)} %bitcast.91, f32[400,1,512]{2,0,1:T(8,128)S(1)} %maximum_convert_fusion, f32[384]{0:T(512)S(1)} %subtract_convert_fusion, f32[]{:T(128)S(6)} %mul.373, ...), kind=kOutput, calls=%fused_computation.15 | convolution fusion | flops 1014497280 | bytes 16781376 | tf_op jit(solution)/shard_map/dot_general | solution.py:76
  178.5 0.0 all-gather.11.cloned.1.call-update
  178.5 0.0 all-gather.13.cloned.1.call-start
  178.6 44.9 %all-gather.11.cloned.1.call-done = bf16[1536,2048]{1,0:T(8,128)(2,1)} async-done(((bf16[384,2048]{1,0:T(8,128)(2,1)}), bf16[1536,2048]{1,0:T(8,128)(2,1)}) %all-gather.11.cloned.1.call-update) | async-done | bytes 6291472 | tf_op jit(solution)/shard_map/all_gather | solution.py:10
  223.5 4.2 %reduce_sum.43 = bf16[384,2048]{1,0:T(8,128)(2,1)S(1)} reduce(bf16[4,384,2048]{2,1,0:T(8,128)(2,1)} %bitcast.80, bf16[]{:T(256)} %constant.87.clone.1), dimensions={0}, to_apply=%region_1.0 | reduce | flops 2359296 | bytes 7864322 | tf_op jit(solution)/shard_map/reduce_sum | solution.py:10
  227.7 0.6 fusion.4
  228.3 2.6 fusion.23
  230.9 3.4 %collective-permute-start.2 = (bf16[8,512]{1,0:T(8,128)(2,1)S(1)}, bf16[8,512]{1,0:T(8,128)(2,1)S(1)}, u32[]{:S(2)}, u32[]{:S(2)}) collective-permute-start(bf16[8,512]{1,0:T(8,128)(2,1)S(1)} %get-tuple-element.5), channel_id=1, source_target_pairs={{0,4},{4,8},{8,12},{1,5},{5,9},{9,13},{2,6},{6,10},{10,14},{3,7},{... | collective-permute-start | bytes 24584 | tf_op jit(solution)/shard_map/ppermute | solution.py:20
  234.3 1.5 collective-permute-start.3
  235.8 0.0 collective-permute-done.2
  235.8 4.1 %collective-permute-done.3 = bf16[8,512]{1,0:T(8,128)(2,1)S(1)} collective-permute-done((bf16[8,512]{1,0:T(8,128)(2,1)S(1)}, bf16[8,512]{1,0:T(8,128)(2,1)S(1)}, u32[]{:S(2)}, u32[]{:S(2)}) %collective-permute-start.3) | collective-permute-done | bytes 8224 | tf_op jit(solution)/shard_map/ppermute | solution.py:21
  239.9 1.0 maximum_convert_fusion.1
  240.9 11.1 %convolution_convert_fusion = bf16[384,2048]{1,0:T(8,128)(2,1)} fusion(bf16[2,512,2048]{2,1,0:T(8,128)(2,1)} %all-gather.9.cloned.1.call-done, bf16[2,1,512,512]{3,2,1,0:T(8,128)(2,1)} %param.9, f32[512]{0:T(512)S(1)} %bitcast.90, f32[400,1,512]{2,0,1:T(8,128)} %maximum_convert_fusion.1, f32[384]{0:T(512)S(1)} %subtract_convert_fusion, f32[]{:T(128)S(6)} %mul.373, ...), kind=kOutput, calls=%fused_computation.14 | convolution fusion | flops 1014497280 | bytes 16780864 | tf_op jit(solution)/shard_map/dot_general | solution.py:76
  252.0 0.0 all-gather.13.cloned.1.call-update
  252.1 45.6 %all-gather.13.cloned.1.call-done = bf16[1536,2048]{1,0:T(8,128)(2,1)} async-done(((bf16[384,2048]{1,0:T(8,128)(2,1)}), bf16[1536,2048]{1,0:T(8,128)(2,1)}) %all-gather.13.cloned.1.call-update) | async-done | bytes 6291472 | tf_op jit(solution)/shard_map/all_gather | solution.py:10
  297.7 5.7 %reduce_sum.45 = bf16[384,2048]{1,0:T(8,128)(2,1)} reduce(bf16[4,384,2048]{2,1,0:T(8,128)(2,1)} %bitcast.81, bf16[]{:T(256)} %constant.87.clone.1), dimensions={0}, to_apply=%region_3.0 | reduce | flops 2359296 | bytes 7864322 | tf_op jit(solution)/shard_map/reduce_sum | solution.py:10
  303.3 3.4 %fusion.7 = bf16[384,2048]{1,0:T(8,128)(2,1)} fusion(bf16[384,2048]{1,0:T(8,128)(2,1)} %reduce_sum.45, bf16[384,2048]{1,0:T(8,128)(2,1)S(1)} %reduce_sum.43, bf16[384,2048]{1,0:T(8,128)(2,1)S(1)} %copy-done), kind=kLoop, calls=%fused_computation.13 | loop fusion | flops 6291456 | bytes 6291456 | tf_op jit(solution)/shard_map/convert_element_type | solution.py:78
  (12 shorter events, 0.1 us)
Async XLA Ops:
  6.5 1.5 copy-start
  6.5 1.9 copy-start.2
  6.5 2.0 copy-start.1
  6.5 85.9 %all-gather.7.cloned.1.call-start = ((), (), s32[]{:S(2)}) async-start(), calls=%async_computation | async-start | bytes 5242880 | tf_op jit(solution)/shard_map/all_gather | solution.py:66
  7.3 166.0 %all-gather.9.cloned.1.call-start = ((), (), s32[]{:S(2)}) async-start(), calls=%async_computation.1 | async-start | bytes 5242880 | tf_op jit(solution)/shard_map/all_gather | solution.py:67
  8.0 215.5 %all-gather.11.cloned.1.call-start = ((), (), s32[]{:S(2)}) async-start(), calls=%async_computation.2 | async-start | bytes 7864320 | tf_op jit(solution)/shard_map/all_gather | solution.py:10
  95.0 2.7 collective-permute-start
  96.3 5.6 %collective-permute-start.1 = (bf16[8,512]{1,0:T(8,128)(2,1)S(1)}, bf16[8,512]{1,0:T(8,128)(2,1)S(1)}, u32[]{:S(2)}, u32[]{:S(2)}) collective-permute-start(bf16[8,512]{1,0:T(8,128)(2,1)S(1)} %get-tuple-element.8), channel_id=1, source_target_pairs={{4,0},{8,4},{12,8},{5,1},{9,5},{13,9},{6,2},{10,6},{14,10},{7,3},{... | collective-permute-start | bytes 24584 | tf_op jit(solution)/shard_map/ppermute | solution.py:21
  178.5 119.2 %all-gather.13.cloned.1.call-start = ((), (), s32[]{:S(2)}) async-start(), calls=%async_computation.3 | async-start | bytes 7864320 | tf_op jit(solution)/shard_map/all_gather | solution.py:10
  230.9 4.9 %collective-permute-start.2 = (bf16[8,512]{1,0:T(8,128)(2,1)S(1)}, bf16[8,512]{1,0:T(8,128)(2,1)S(1)}, u32[]{:S(2)}, u32[]{:S(2)}) collective-permute-start(bf16[8,512]{1,0:T(8,128)(2,1)S(1)} %get-tuple-element.5), channel_id=1, source_target_pairs={{0,4},{4,8},{8,12},{1,5},{5,9},{9,13},{2,6},{6,10},{10,14},{3,7},{... | collective-permute-start | bytes 24584 | tf_op jit(solution)/shard_map/ppermute | solution.py:20
  234.3 5.5 %collective-permute-start.3 = (bf16[8,512]{1,0:T(8,128)(2,1)S(1)}, bf16[8,512]{1,0:T(8,128)(2,1)S(1)}, u32[]{:S(2)}, u32[]{:S(2)}) collective-permute-start(bf16[8,512]{1,0:T(8,128)(2,1)S(1)} %get-tuple-element.6), channel_id=1, source_target_pairs={{4,0},{8,4},{12,8},{5,1},{9,5},{13,9},{6,2},{10,6},{14,10},{7,3},{... | collective-permute-start | bytes 24584 | tf_op jit(solution)/shard_map/ppermute | solution.py:21
Sparse Core Ops, SparseCore 0:
  8.9 83.4 all-gather.6
  94.0 79.2 all-gather.8
  178.6 44.8 all-gather.10
  252.2 45.4 all-gather.12
